TPU v7x, 32 devices: a whole 2x2x4 slice. The times are simulated.
32 devices in a mesh: ep: 8 (over z, core), tp: 4 (over y, x).
Axes of the slice: x: 2, y: 2, z: 4, core: 2. Of those that a mesh axis runs over, the one named last changes fastest.
Arguments:
- attn_rows: bfloat16 [1024, 2048], P('ep'), may hold values from -6 to 6
- attn_gain: float32 [2048], replicated, may hold values from 0.1 to 1.9
- query_weight: bfloat16 [2048, 1024], P(None, 'tp'), may hold values from -0.125 to 0.125
- key_weight: bfloat16 [2048, 1024], P(None, 'tp'), may hold values from -0.125 to 0.125
- value_weight: bfloat16 [2048, 1024], P(None, 'tp'), may hold values from -0.125 to 0.125
- key_bias: bfloat16 [16, 1024], P('tp', 'ep'), may hold values from -14 to 0
- out_weight: bfloat16 [1024, 2048], P(None, 'tp'), may hold values from -0.75 to 0.75
- expert_rows: bfloat16 [1024, 2048], P('ep'), may hold values from -6 to 6
- expert_gain: float32 [2048], replicated, may hold values from 0.1 to 1.9
- expert_ids: int32 [1024, 2], P('ep'), may hold values from 0 to 31, all different within a row; in each aligned block of 128 rows (0 to 127, 128 to 255, ...) at most 16 rows name the same one
- group_logits: float32 [1024, 4], P('ep'), may hold values from -6 to 6
- pair_logits: float32 [1024, 2], P('ep'), may hold values from -6 to 6
- gate_weight: bfloat16 [32, 2048, 2048], P('ep', None, 'tp'), may hold values from -0.125 to 0.125
- up_weight: bfloat16 [32, 2048, 2048], P('ep', None, 'tp'), may hold values from -0.125 to 0.125
- down_weight: bfloat16 [32, 2048, 2048], P('ep', None, 'tp'), may hold values from -0.125 to 0.125
Outputs:
- mixed: bfloat16 [1024, 2048], P('ep', 'tp')
- expert_out: bfloat16 [1024, 2048], P('ep', 'tp')
Inputs may be any that keep to these rules, and one draw needn't show every extreme that they name: `expert_ids`: each row names two different experts; in every aligned block of 128 rows no expert is named more than 16 times.
All inputs are finite; a program needn't handle non-finite values.
Results may differ from a plain program's by a relative error of at most 0.0083.
Values may be sent and summed in bfloat16 or wider, within the bound.
A program may use at most 64 MiB of HBM per device.

v0:
```python
import jax
import jax.numpy as jnp
from jax import lax
from jax.sharding import PartitionSpec as P

EXPERTS = 32
GROUPS = 4
GROUP_SIZE = 8
CAP = 16


epsilon = 1e-06


def norm_rows(rows, gain):
    values = rows.astype(jnp.float32)
    scaled = values * lax.rsqrt(jnp.mean(values * values, axis=-1, keepdims=True) + epsilon)
    return (scaled * gain).astype(jnp.bfloat16)


def shards(
    attn_rows,
    attn_gain,
    query_weight,
    key_weight,
    value_weight,
    key_bias,
    out_weight,
    expert_rows,
    expert_gain,
    expert_ids,
    group_logits,
    pair_logits,
    gate_weight,
    up_weight,
    down_weight,
):
    rows_dev = attn_rows.shape[0]
    blocks = lax.axis_size("ep")
    own_start = lax.axis_index("ep") * rows_dev
    heads_local = key_bias.shape[0]
    head_size = query_weight.shape[1] // heads_local
    width_local = heads_local * head_size
    scale = head_size ** (-0.5)
    normed = norm_rows(attn_rows, attn_gain)
    query = jnp.dot(normed, query_weight, preferred_element_type=jnp.float32).astype(jnp.bfloat16)
    query = query.reshape(rows_dev, heads_local, head_size)
    keys = jnp.dot(normed, key_weight, preferred_element_type=jnp.float32).astype(jnp.bfloat16)
    values = jnp.dot(normed, value_weight, preferred_element_type=jnp.float32).astype(jnp.bfloat16)
    pairs = jnp.concatenate([keys, values], axis=1)
    bias_rows = key_bias.T
    query_pos = own_start + jnp.arange(rows_dev)
    init = (
        jnp.zeros((blocks, heads_local, rows_dev), jnp.float32),
        jnp.zeros((blocks, heads_local, rows_dev, head_size), jnp.float32),
    )
    piece = (
        lax.all_gather(pairs, "ep", axis=0, tiled=True),
        lax.all_gather(bias_rows, "ep", axis=0, tiled=True),
    )

    def work(state):
        pair_rows, bias_piece = piece
        count = pair_rows.shape[0]
        spans = count // rows_dev
        key_part = pair_rows[:, :width_local].reshape(count, heads_local, head_size)
        value_part = pair_rows[:, width_local:].reshape(spans, rows_dev, heads_local, head_size)
        scores = (
            jnp.einsum("thd,shd->hts", query, key_part, preferred_element_type=jnp.float32) * scale
        )
        scores = scores + bias_piece.T.astype(jnp.float32)[:, None, :]
        scores = scores.reshape(heads_local, rows_dev, spans, rows_dev)
        causal = jnp.arange(count)[None, :] < query_pos[:, None]
        causal = causal.reshape(rows_dev, spans, rows_dev)
        negative_part = jax.nn.log_sigmoid(-scores)
        log_keep = jnp.where(causal, negative_part, 0.0)
        suffix = lax.cumsum(log_keep, axis=3, reverse=True) - log_keep
        weights = jnp.where(causal, jnp.exp(scores + negative_part + suffix), 0.0).astype(
            jnp.bfloat16
        )
        block_out = jnp.einsum(
            "htnr,nrhd->nhtd", weights, value_part, preferred_element_type=jnp.float32
        )
        block_keep = jnp.transpose(jnp.sum(log_keep, axis=3), (2, 0, 1))
        return (block_keep, block_out)

    def untouched(state):
        return state

    totals, outputs = lax.cond(jnp.int32(0) < own_start + rows_dev, work, untouched, init)
    later = lax.cumsum(totals, axis=0, reverse=True) - totals
    merged = jnp.sum(jnp.exp(later)[..., None] * outputs, axis=0)
    attended = jnp.transpose(merged, (1, 0, 2)).reshape(rows_dev, width_local).astype(jnp.bfloat16)
    mixed = jnp.dot(
        lax.all_gather(attended, "tp", axis=1, tiled=True),
        out_weight,
        preferred_element_type=jnp.float32,
    )
    mixed = mixed.astype(jnp.bfloat16)
    normed = norm_rows(expert_rows, expert_gain)
    width = normed.shape[1]
    cols_local = down_weight.shape[2]
    flattened = expert_ids.reshape(-1)
    picks = flattened.shape[0]
    marks = (flattened[:, None] == jnp.arange(EXPERTS)[None, :]).astype(jnp.int32)
    position = jnp.sum((jnp.cumsum(marks, axis=0) - marks) * marks, axis=1)
    source = jnp.arange(picks) // 2
    send = (
        jnp.zeros((EXPERTS, CAP, width), jnp.bfloat16).at[flattened, position].set(normed[source])
    )
    send = send.reshape(blocks, EXPERTS // blocks, CAP, width)
    shares = jnp.exp(group_logits)
    shares = shares / jnp.sum(shares, axis=1, keepdims=True)
    groups = expert_ids // GROUP_SIZE
    group_marks = (groups[:, :, None] == jnp.arange(GROUPS)[None, None, :]).astype(jnp.float32)
    chosen = jnp.sum(shares[:, None, :] * group_marks, axis=2)
    spread = pair_logits[:, 0] - pair_logits[:, 1]
    pair_share = jnp.stack([jax.nn.sigmoid(spread), jax.nn.sigmoid(-spread)], axis=1)
    route_weights = chosen * pair_share
    arrived = lax.all_to_all(send, "ep", split_axis=0, concat_axis=0, tiled=True)
    gate = jnp.einsum("secd,edf->secf", arrived, gate_weight, preferred_element_type=jnp.float32)
    up = jnp.einsum("secd,edf->secf", arrived, up_weight, preferred_element_type=jnp.float32)
    hidden = (jax.nn.silu(gate) * up).astype(jnp.bfloat16)
    result = jnp.einsum(
        "secf,efd->secd",
        lax.all_gather(hidden, "tp", axis=3, tiled=True),
        down_weight,
        preferred_element_type=jnp.float32,
    ).astype(jnp.bfloat16)
    back = lax.all_to_all(result, "ep", split_axis=0, concat_axis=0, tiled=True).reshape(
        EXPERTS, CAP, cols_local
    )
    picked = back[flattened, position].reshape(expert_rows.shape[0], 2, cols_local)
    combined = jnp.sum(route_weights[:, :, None] * picked.astype(jnp.float32), axis=1)
    expert_out = combined.astype(jnp.bfloat16)
    return (mixed, expert_out)


def solution(mesh):
    placed = (
        P("ep", None),
        P(),
        P(None, "tp"),
        P(None, "tp"),
        P(None, "tp"),
        P("tp", "ep"),
        P(None, "tp"),
        P("ep", None),
        P(),
        P("ep", None),
        P("ep", None),
        P("ep", None),
        P("ep", None, "tp"),
        P("ep", None, "tp"),
        P("ep", None, "tp"),
    )
    return jax.shard_map(
        shards,
        mesh=mesh,
        in_specs=placed,
        out_specs=(P("ep", "tp"), P("ep", "tp")),
        check_vma=False,
    )
```

profile of v0, /device:TPU:0, one launch (start us, length us, event | category | flops | bytes accessed | tf_op | source)
XLA Modules:
  0.0 217.6 jit_solution(6197130327097022575)
XLA Ops:
  7.2 0.9 copy.83
  8.5 0.6 reduce-window.6
  9.4 1.2 fusion.48
  10.7 1.2 fusion.50
  12.0 2.3 %gather_fusion = bf16[256,2048]{1,0:T(8,128)(2,1)} fusion(bf16[128,2048]{1,0:T(8,128)(2,1)S(1)} %fusion.50, s32[1024]{0:T(1024)S(1)} %pad_clamp_fusion), kind=kCustom, calls=%fused_computation | custom fusion | bytes 2098176 | tf_op jit(solution)/shard_map/gather | solution.py:109
  14.6 33.3 %scatter_fusion = bf16[32,16,2048]{2,1,0:T(8,128)(2,1)S(1)} fusion(bf16[32,16,2048]{2,1,0:T(8,128)(2,1)S(1)} %broadcast_in_dim.19, s32[256]{0:T(256)S(1)} %bitcast.90, bf16[256,2048]{1,0:T(8,128)(2,1)} %gather_fusion), kind=kCustom, calls=%fused_computation.2 | custom fusion | bytes 3147776 | tf_op jit(solution)/shard_map/scatter | solution.py:109
  47.9 55.5 %all_to_all.10 = bf16[8,4,16,2048]{3,2,1,0:T(8,128)(2,1)S(1)} all-to-all(bf16[8,4,16,2048]{3,2,1,0:T(8,128)(2,1)S(1)} %bitcast.89), channel_id=1, replica_groups=mesh['ep'=8,'tp'=4] {'ep'}, dimensions={0} | all-to-all | bytes 4194304 | tf_op jit(solution)/shard_map/all_to_all | solution.py:120
  103.3 4.8 %fusion.19 = f32[8,4,16,512]{3,2,0,1:T(8,128)S(1)} fusion(bf16[4,2048,512]{2,1,0:T(8,128)(2,1)} %param.29, bf16[8,4,16,2048]{3,2,1,0:T(8,128)(2,1)S(1)} %all_to_all.10), kind=kOutput, calls=%fused_computation.27 | convolution fusion | flops 1073741824 | bytes 11534336 | tf_op jit(solution)/shard_map/secd,edf->secf/dot_general | solution.py:121
  108.2 2.2 fusion.34
  111.1 0.6 copy-done.8
  111.7 0.4 convolution_convert_fusion.2
  112.0 0.7 pad_maximum_fusion
  113.0 9.7 %all_gather.13 = bf16[1024,4]{0,1:T(4,128)(2,1)S(1)} all-gather(bf16[128,4]{0,1:T(4,128)(2,1)S(1)} %bitcast.100), channel_id=1, replica_groups=mesh['ep'=8,'tp'=4] {'ep'}, dimensions={0}, use_global_device_ids=true | all-gather | bytes 9216 | tf_op jit(solution)/shard_map/all_gather | solution.py:59
  122.7 21.8 %all-gather.5.cloned.1.call-done = bf16[8,4,16,2048]{3,2,0,1:T(8,128)(2,1)} async-done(((bf16[8,4,16,512]{3,2,0,1:T(8,128)(2,1)}), bf16[8,4,16,2048]{3,2,0,1:T(8,128)(2,1)}) %all-gather.5.cloned.1.call-update) | async-done | bytes 2097168 | tf_op jit(solution)/shard_map/all_gather | solution.py:126
  144.5 5.3 %fusion.42 = bf16[8,4,16,512]{3,2,0,1:T(8,128)(2,1)S(1)} fusion(bf16[8,4,16,2048]{3,2,0,1:T(8,128)(2,1)} %all-gather.5.cloned.1.call-done, bf16[4,2048,512]{2,1,0:T(8,128)(2,1)} %param.31), kind=kOutput, calls=%fused_computation.36 | convolution fusion | flops 1074003968 | bytes 11010048 | tf_op jit(solution)/shard_map/secf,efd->secd/dot_general | solution.py:124
  149.8 0.9 copy.89
  150.7 4.6 %all-to-all-start.1 = ((bf16[8,4,16,512]{3,2,1,0:T(8,128)(2,1)}), bf16[8,4,16,512]{3,2,1,0:T(8,128)(2,1)}, u32[]{:S(2)}, u32[]{:S(2)}) async-start(bf16[8,4,16,512]{3,2,1,0:T(8,128)(2,1)} %copy.89), calls=%async_computation.1 | async-start | bytes 1048576 | tf_op jit(solution)/shard_map/all_to_all | solution.py:130
  155.6 19.5 %all-gather.3.cloned.1.call-done = bf16[1024,512]{1,0:T(8,128)(2,1)} async-done(((bf16[128,512]{1,0:T(8,128)(2,1)}), bf16[1024,512]{1,0:T(8,128)(2,1)}) %all-gather.3.cloned.1.call-update) | async-done | bytes 1048592 | tf_op jit(solution)/shard_map/all_gather | solution.py:58
  175.2 17.9 %conditional.1 = (f32[8,4,128]{2,0,1:T(8,128)S(1)}, f32[8,4,128,64]{2,3,1,0:T(8,128)}) conditional(s32[]{:T(128)} %convert_element_type.71, () %tuple.16, (s32[]{:T(128)}, s32[128]{0:T(128)S(1)}, bf16[128,256]{1,0:T(8,128)(2,1)S(1)}, bf16[1024,512]{1,0:T(8,128)(2,1)}, bf16[1024,4]{0,1:T(4,128)(2,1)S(1)}) %tuple.17), branch_computations={%region_1.0_spmd, %region_2.5_spmd} | conditional | flops 217712768 | bytes 26871344 | solution.py:90
  175.3 1.5 copy.80
  176.8 0.9 slice_bitcast_fusion
  177.6 0.5 multiply_add_fusion
  178.1 1.8 copy.93
  179.9 2.2 %copy.71 = f32[4,128,8,128]{1,2,3,0:T(8,128)S(1)} copy(f32[4,128,8,128]{3,2,1,0:T(8,128)} %bitcast.93) | data formatting | bytes 4194304 | tf_op jit(solution)/shard_map/cond/branch_1_fun/reshape | solution.py:72
  182.4 1.3 fusion.6
  183.7 7.7 %select_convert_fusion = bf16[4,128,8,128]{1,2,3,0:T(8,128)(2,1)S(1)} fusion(f32[4,128,8,128]{1,2,3,0:T(8,128)S(1)} %copy.71, pred[128,8,128]{0,1,2:T(8,128)(4,1)S(1)} %broadcast_compare_fusion), kind=kOutput, calls=%fused_computation.5 | output fusion | flops 77594624 | bytes 3276800 | tf_op jit(solution)/shard_map/cond/branch_1_fun/reduce_window_sum | solution.py:77
  191.6 1.5 fusion.2
  193.1 1.3 multiply_reduce_fusion
  194.5 10.7 %all_gather.14 = bf16[128,1024]{0,1:T(8,128)(2,1)S(1)} all-gather(bf16[128,256]{0,1:T(8,128)(2,1)S(1)} %bitcast.96), channel_id=1, replica_groups=mesh['ep'=8,'tp'=4] {'tp'}, dimensions={1}, use_global_device_ids=true | all-gather | bytes 327680 | tf_op jit(solution)/shard_map/all_gather | solution.py:95
  205.2 1.0 convolution_convert_fusion
  206.2 2.9 %gather_fusion.1 = bf16[256,512]{1,0:T(8,128)(2,1)S(1)} fusion(bf16[32,16,512]{2,1,0:T(8,128)(2,1)} %bitcast.21, s32[256]{0:T(256)S(1)} %bitcast.91), kind=kCustom, calls=%fused_computation.1 | custom fusion | bytes 526336 | tf_op jit(solution)/shard_map/gather | solution.py:133
  209.4 1.4 multiply_reduce_fusion.1
  (66 shorter events, 3.1 us)
Async XLA Ops:
  7.2 198.0 %copy-start = (bf16[1024,512]{1,0:T(8,128)(2,1)S(1)}, bf16[1024,512]{1,0:T(8,128)(2,1)}, u32[]{:S(2)}) copy-start(bf16[1024,512]{1,0:T(8,128)(2,1)} %param.23) | copy-start | bytes 3145732
  7.2 137.3 %all-gather.5.cloned.1.call-start = ((), (), s32[]{:S(2)}) async-start(), calls=%async_computation.3 | async-start | bytes 2621440 | tf_op jit(solution)/shard_map/all_gather | solution.py:126
  47.9 60.3 %slice-start = ((s8[8388608]{0:T(1024)(128)(4,1)}), s8[4194304]{0:T(1024)(128)(4,1)S(1)}, s32[]{:S(2)}) async-start(s8[8388608]{0:T(1024)(128)(4,1)} %bitcast.102), calls=%async_computation.4 | async-start | bytes 8388608
  103.3 4.8 %slice-start.1 = ((s8[8388608]{0:T(1024)(128)(4,1)}), s8[4194304]{0:T(1024)(128)(4,1)S(1)}, s32[]{:S(2)}) async-start(s8[8388608]{0:T(1024)(128)(4,1)} %bitcast.102), calls=%async_computation.5 | async-start | bytes 8388608
  108.2 2.3 %copy-start.2 = (bf16[128,2048]{1,0:T(8,128)(2,1)S(1)}, bf16[128,2048]{1,0:T(8,128)(2,1)}, u32[]{:S(2)}) copy-start(bf16[128,2048]{1,0:T(8,128)(2,1)} %param.17) | copy-start | bytes 1572868
  108.2 2.5 %copy-start.7 = (bf16[2048,256]{1,0:T(8,128)(2,1)S(1)}, bf16[2048,256]{1,0:T(8,128)(2,1)}, u32[]{:S(2)}) copy-start(bf16[2048,256]{1,0:T(8,128)(2,1)} %param.21) | copy-start | bytes 3145732
  108.2 2.5 %copy-start.10 = (f32[2048]{0:T(1024)S(1)}, f32[2048]{0:T(1024)}, u32[]{:S(2)}) copy-start(f32[2048]{0:T(1024)} %param.18) | copy-start | bytes 24580
  110.4 64.8 %all-gather.3.cloned.1.call-start = ((), (), s32[]{:S(2)}) async-start(), calls=%async_computation.2 | async-start | bytes 1179648 | tf_op jit(solution)/shard_map/all_gather | solution.py:58
  110.4 1.2 copy-start.8
  110.6 2.1 copy-start.4
  110.6 2.1 copy-start.3
  110.7 2.2 copy-start.6
  110.7 2.3 %copy-start.5 = (bf16[4,128]{1,0:T(4,128)(2,1)S(1)}, bf16[4,128]{1,0:T(4,128)(2,1)}, u32[]{:S(2)}) copy-start(bf16[4,128]{1,0:T(4,128)(2,1)} %param.22) | copy-start | bytes 3076
  149.8 5.5 %copy-start.9 = (bf16[2048,256]{1,0:T(8,128)(2,1)S(1)}, bf16[2048,256]{1,0:T(8,128)(2,1)}, u32[]{:S(2)}) copy-start(bf16[2048,256]{1,0:T(8,128)(2,1)} %param.19) | copy-start | bytes 3145732
  150.7 55.5 %all-to-all-start.1 = ((bf16[8,4,16,512]{3,2,1,0:T(8,128)(2,1)}), bf16[8,4,16,512]{3,2,1,0:T(8,128)(2,1)}, u32[]{:S(2)}, u32[]{:S(2)}) async-start(bf16[8,4,16,512]{3,2,1,0:T(8,128)(2,1)} %copy.89), calls=%async_computation.1 | async-start | bytes 1048576 | tf_op jit(solution)/shard_map/all_to_all | solution.py:130
  183.7 7.8 %copy-start.1 = (bf16[32,8,8,128]{3,1,2,0:T(8,128)(2,1)S(1)}, bf16[32,8,8,128]{3,1,2,0:T(8,128)(2,1)}, u32[]{:S(2)}) copy-start(bf16[32,8,8,128]{3,1,2,0:T(8,128)(2,1)} %get-tuple-element.46) | copy-start | bytes 1572868 | tf_op jit(solution)/shard_map/cond
Sparse Core Ops, SparseCore 0:
  110.5 33.9 all-gather.4
  146.7 28.4 all-gather.2
where the time goes:
time: 219 us; the launch traced here: 218 us
  blocking collectives  75.8 us (35%)
  local copies, waits for them, and re-layouts  48.8 us (22%)
  waiting for transfers between devices  41.4 us (19%)
  other arithmetic  16.2 us (7%)
  matrix products  16.2 us (7%)
  between operations  14.4 us (7%)
  starting transfers between devices  4.69 us (2%)
    all_to_all x1, blocking collectives, shards(): lax.all_to_all(send, 'ep', split_axis=0, concat_axis=0, tiled=True)  55.5 us
    scatter x1, local copies, waits for them, and re-layouts, shards(): jnp.zeros((EXPERTS, CAP, width), jnp.bfloat16).at[flattened, position]  33.3 us
    all_gather x1, waiting for transfers between devices, shards(): lax.all_gather(hidden, 'tp', axis=3, tiled=True)  21.8 us
    all_gather x1, waiting for transfers between devices, shards(): lax.all_gather(pairs, 'ep', axis=0, tiled=True)  19.5 us
    all_gather x1, blocking collectives, shards(): lax.all_gather(attended, 'tp', axis=1, tiled=True)  10.7 us
    all_gather x1, blocking collectives, shards(): lax.all_gather(bias_rows, 'ep', axis=0, tiled=True)  9.7 us
    another operation x1, other arithmetic, work(): suffix = lax.cumsum(log_keep, axis=3, reverse=True) - log_keep  7.74 us
    dot_general x1, matrix products, shards(): jnp.einsum('secf,efd->secd', lax.all_gather(hidden, 'tp', axis=3, tiled=T...  5.28 us
  transfers between devices with their start and end apart: 3, of which 2 were waited for; matrix products, arithmetic and copies ran while one was open for 13% of the time, Pallas kernels for 0%

commit v1 on v0

v1 whole, which is shorter than its diff:
```python
import functools

import jax
import jax.numpy as jnp
from jax import lax
from jax.experimental import pallas as pl
from jax.experimental.pallas import tpu as pltpu
from jax.sharding import PartitionSpec as P

MESH = pl.DeviceIdType.MESH
CAP = 16
GROUPS = 4
GROUP_SIZE = 8
BIAS_ROW = 8
epsilon = 1e-06
f32 = jnp.float32
bf16 = jnp.bfloat16


def dot(a, b):
    return jnp.dot(a, b, preferred_element_type=f32)


def loop(n, body, start=0):
    def step(i, carry):
        body(i)
        return carry

    lax.fori_loop(start, n, step, 0)


def kernel(
    E,
    T,
    rows_ref,
    again_ref,
    wq_hbm,
    wk_hbm,
    wv_hbm,
    meta_ref,
    wo_hbm,
    erows_hbm,
    egain_ref,
    ids_ref,
    glog_ref,
    plog_ref,
    wg_hbm,
    wu_hbm,
    wd_hbm,
    mixed_ref,
    out_ref,
    wqkv,
    wo,
    wg,
    wu,
    wd,
    X,
    XG,
    HB,
    M,
    KV,
    Q,
    AT,
    RES,
    RB,
    s_w,
    s_wg,
    s_wu,
    s_wd,
    s_lx,
    tx_z,
    tx_tp,
    tx_d,
    rx,
    tx_m,
    rx_m,
    tx_kv,
    tx_kvd,
    rx_kv,
    tx_h,
    rx_h,
    tx_a,
    rx_a,
    tx_r,
    rx_r,
):
    Z = E // 2
    R, D = rows_ref.shape
    W = wq_hbm.shape[1]
    DQ = X.shape[3]
    EL = wg.shape[0]
    FL = wg.shape[2]
    e = lax.axis_index("ep")
    t = lax.axis_index("tp")
    z = e // 2
    c = e % 2
    mate = 2 * z + (1 - c)
    HD = Q.shape[2]
    heads = Q.shape[0]
    scale = HD ** (-0.5)

    def remote(src, dst, ssem, rsem, de, dt):
        return pltpu.make_async_remote_copy(
            src_ref=src,
            dst_ref=dst,
            send_sem=ssem,
            recv_sem=rsem,
            device_id=(de, dt),
            device_id_type=MESH,
        )

    w_copies = [
        pltpu.make_async_copy(wk_hbm, wqkv.at[:, pl.ds(0, W)], s_w.at[0]),
        pltpu.make_async_copy(wv_hbm, wqkv.at[:, pl.ds(W, W)], s_w.at[1]),
        pltpu.make_async_copy(wq_hbm, wqkv.at[:, pl.ds(2 * W, W)], s_w.at[2]),
    ] if W % 128 == 0 else [
        pltpu.make_async_copy(wk_hbm, wqkv.at[0], s_w.at[0]),
        pltpu.make_async_copy(wv_hbm, wqkv.at[1], s_w.at[1]),
        pltpu.make_async_copy(wq_hbm, wqkv.at[2], s_w.at[2]),
    ]
    wo_copy = pltpu.make_async_copy(wo_hbm, wo, s_w.at[3])
    x_copies = [
        pltpu.make_async_copy(erows_hbm.at[:, pl.ds(q * DQ, DQ)], X.at[e, q], s_lx.at[q])
        for q in range(T)
    ]

    def wg_copy(i):
        return pltpu.make_async_copy(wg_hbm.at[i], wg.at[i], s_wg.at[i])

    def wu_copy(i):
        return pltpu.make_async_copy(wu_hbm.at[i], wu.at[i], s_wu.at[i])

    def wd_copy(i):
        return pltpu.make_async_copy(wd_hbm.at[i], wd.at[i], s_wd.at[i])

    for cp in x_copies + w_copies:
        cp.start()

    def start_gu(i):
        wg_copy(i).start()
        wu_copy(i).start()

    loop(EL, start_gu)
    loop(EL, lambda i: wd_copy(i).start())
    wo_copy.start()

    barrier = pltpu.get_barrier_semaphore()

    def greet_ep(d):
        pl.semaphore_signal(
            barrier, inc=1, device_id=((e + d) % E, t), device_id_type=MESH
        )

    def greet_tp(d):
        pl.semaphore_signal(
            barrier, inc=1, device_id=(e, (t + d) % T), device_id_type=MESH
        )

    loop(E, greet_ep, 1)
    loop(T, greet_tp, 1)
    pl.semaphore_wait(barrier, E - 1 + T - 1)

    for cp in x_copies:
        cp.wait()

    def z_copy(d):
        return remote(
            X.at[e, t], X.at[e, t], tx_z.at[d], rx.at[e, t], 2 * ((z + d) % Z) + c, t
        )

    def mate_copy(s, q):
        return remote(X.at[s, q], X.at[s, q], tx_d.at[s, q], rx.at[s, q], mate, t)

    def tp_copy(s, j):
        return remote(
            X.at[s, t], X.at[s, t], tx_tp.at[s, j], rx.at[s, t], e, (t + j) % T
        )

    def meta_copy(d):
        return remote(meta_ref, M.at[e], tx_m.at[d], rx_m.at[e], (e + d) % E, t)

    def kv_copy(d):
        return remote(
            KV.at[e], KV.at[e], tx_kv.at[d], rx_kv.at[e], 2 * ((z + d) % Z) + c, t
        )

    def kv_mate(s):
        return remote(KV.at[s], KV.at[s], tx_kvd.at[s], rx_kv.at[s], mate, t)

    def x_arrived(s, q):
        mate_copy(s, q).wait_recv()

    loop(E, lambda d: meta_copy(d).start(), 1)
    loop(Z, lambda d: z_copy(d).start(), 1)
    loop(T, lambda q: mate_copy(e, q).start())
    M[e] = meta_ref[...]

    values = rows_ref[...].astype(f32)
    scaled = values * lax.rsqrt(jnp.mean(values * values, axis=-1, keepdims=True) + epsilon)
    normed = (scaled * again_ref[...]).astype(bf16)
    for cp in w_copies:
        cp.wait()
    if W % 128 == 0:
        KV[e] = dot(normed, wqkv[:, : 2 * W]).astype(bf16)
    else:
        KV[e] = jnp.concatenate([dot(normed, wqkv[0]), dot(normed, wqkv[1])], axis=1).astype(bf16)

    def kv_send(d):
        @pl.when((z + d) % Z > z)
        def _():
            kv_copy(d).start()

    loop(Z, kv_send, 1)

    @pl.when(c == 0)
    def _():
        kv_mate(e).start()

    query = dot(normed, wqkv[:, 2 * W :] if W % 128 == 0 else wqkv[2]).astype(bf16)
    for h in range(heads):
        Q[h] = query[:, h * HD : (h + 1) * HD]

    def relay(d):
        s = 2 * ((z + d) % Z) + c
        x_arrived(s, t)
        loop(T, lambda j: tp_copy(s, j).start(), 1)
        mate_copy(s, t).start()

    loop(Z, relay, 1)

    row_i = lax.broadcasted_iota(jnp.int32, (R, R), 0)
    col_i = lax.broadcasted_iota(jnp.int32, (R, R), 1)
    before = (row_i < col_i).astype(f32).astype(bf16)
    after = (row_i > col_i).astype(f32).astype(bf16)
    slots = EL * CAP
    slot_i = lax.broadcasted_iota(jnp.int32, (slots, R), 0)
    slot_expert = (slot_i // CAP + e * EL).astype(f32)
    slot_place = (slot_i % CAP).astype(f32)

    def pick(s):
        names = M[s]
        mark = (names[0:1, :] == slot_expert) | (names[1:2, :] == slot_expert)
        place = dot(mark.astype(f32).astype(bf16), before)
        take = (mark & (place == slot_place)).astype(f32).astype(bf16)
        raw = [dot(take, X[s, q]) for q in range(T)]
        square = sum(jnp.sum(part * part, axis=1, keepdims=True) for part in raw)
        factor = lax.rsqrt(square / D + epsilon)
        for q in range(T):
            part = (raw[q] * factor * egain_ref[:, q * DQ : (q + 1) * DQ]).astype(bf16)
            for i in range(EL):
                XG[i, s, :, pl.ds(q * DQ, DQ)] = part[i * CAP : (i + 1) * CAP]

    loop(E, lambda d: remote(meta_ref, M.at[(e + d) % E], tx_m.at[0], rx_m.at[(e + d) % E], e, t).wait_recv(), 1)
    pick(e)

    def mate_rows(s):
        loop(T, lambda q: x_arrived(s, q))
        pick(s)

    mate_rows(mate)

    def kv_relay(s):
        kv_mate(s).wait_recv()
        kv_mate(s).start()

    loop(z, lambda k: kv_relay(2 * k + c))

    def spread(d):
        s = 2 * ((z + d) % Z) + c

        def on(j):
            q = (t + j) % T
            x_arrived(s, q)
            mate_copy(s, q).start()

        loop(T, on, 1)
        pick(s)

    loop(Z, spread, 1)
    loop(Z, lambda d: mate_rows(2 * ((z + d) % Z) + (1 - c)), 1)

    def h_copy(i, j):
        return remote(
            HB.at[t, i], HB.at[t, i], tx_h.at[i, j], rx_h.at[i, t], e, (t + j) % T
        )

    def hidden(i):
        rows = XG[i].reshape(E * CAP, D)
        wg_copy(i).wait()
        gate = dot(rows, wg[i])
        wu_copy(i).wait()
        up = dot(rows, wu[i])
        HB[t, i] = (jax.nn.silu(gate) * up).astype(bf16)
        loop(T, lambda j: h_copy(i, j).start(), 1)

    loop(EL, hidden)

    loop(z, lambda k: kv_mate(2 * k + (1 - c)).wait_recv())

    @pl.when(c == 1)
    def _():
        kv_mate(mate).wait_recv()

    def block(j, carry):
        s = e - j
        causal = col_i + s * R < row_i + e * R
        new = []
        for h in range(heads):
            later, total = carry[h]
            key = KV[s, :, pl.ds(h * HD, HD)]
            value = KV[s, :, pl.ds(W + h * HD, HD)]
            score = lax.dot_general(
                Q[h], key, (((1,), (1,)), ((), ())), preferred_element_type=f32
            )
            score = score * scale + M[s, pl.ds(BIAS_ROW + h, 1), :]
            negative = -(jnp.maximum(score, 0.0) + jnp.log1p(jnp.exp(-jnp.abs(score))))
            keep = jnp.where(causal, negative, 0.0)
            high = keep.astype(bf16)
            low = (keep - high.astype(f32)).astype(bf16)
            suffix = dot(high, after) + dot(low, after)
            weight = jnp.where(causal, jnp.exp(score + negative + suffix), 0.0).astype(bf16)
            total = total + jnp.exp(later) * dot(weight, value)
            later = later + suffix[:, 0:1] + keep[:, 0:1]
            new.append((later, total))
        return tuple(new)

    init = tuple(
        (jnp.zeros((R, 1), f32), jnp.zeros((R, HD), f32)) for _ in range(heads)
    )
    merged = lax.fori_loop(0, e + 1, block, init)
    AT[t] = jnp.concatenate([total for _, total in merged], axis=1).astype(bf16)

    def a_copy(j):
        return remote(AT.at[t], AT.at[t], tx_a.at[j], rx_a.at[t], e, (t + j) % T)

    loop(T, lambda j: a_copy(j).start(), 1)

    def r_copy(i, d):
        s = (e + d) % E
        return remote(RES.at[s, i], RB.at[e, i], tx_r.at[i, d], rx_r.at[e, i], s, t)

    def down(i):
        wd_copy(i).wait()

        def arrived(j):
            q = (t + j) % T
            remote(HB.at[q, i], HB.at[q, i], tx_h.at[i, 0], rx_h.at[i, q], e, t).wait_recv()

        loop(T, arrived, 1)
        result = dot(HB[0, i], wd[i, pl.ds(0, FL), :])
        for q in range(1, T):
            result = result + dot(HB[q, i], wd[i, pl.ds(q * FL, FL), :])
        result = result.astype(bf16).reshape(E, CAP, result.shape[1])
        RES[:, i] = result
        RB[e, i] = RES[e, i]
        loop(E, lambda d: r_copy(i, d).start(), 1)

    loop(EL, down)

    wo_copy.wait()

    def a_arrived(j):
        q = (t + j) % T
        remote(AT.at[q], AT.at[q], tx_a.at[0], rx_a.at[q], e, t).wait_recv()

    loop(T, a_arrived, 1)
    mixed = dot(AT[0], wo[pl.ds(0, W), :])
    for q in range(1, T):
        mixed = mixed + dot(AT[q], wo[pl.ds(q * W, W), :])
    mixed_ref[...] = mixed.astype(bf16)

    experts = E * EL
    ids = [ids_ref[:, k : k + 1] for k in range(2)]
    expert_i = lax.broadcasted_iota(jnp.int32, (R, experts), 1)
    named = (expert_i == ids[0]) | (expert_i == ids[1])
    places = dot(after, named.astype(f32).astype(bf16))
    shares = jnp.exp(glog_ref[...])
    shares = shares / jnp.sum(shares, axis=1, keepdims=True)
    group_i = lax.broadcasted_iota(jnp.int32, shares.shape, 1)
    back_i = lax.broadcasted_iota(jnp.int32, (R, experts * CAP), 1)
    pair = plog_ref[...]
    takes, shares_k = [], []
    for k in range(2):
        own = jnp.sum(jnp.where(expert_i == ids[k], places, 0.0), axis=1, keepdims=True)
        takes.append((back_i == ids[k] * CAP + own.astype(jnp.int32)).astype(f32).astype(bf16))
        chosen = jnp.sum(jnp.where(group_i == ids[k] // GROUP_SIZE, shares, 0.0), axis=1, keepdims=True)
        spread_k = pair[:, k : k + 1] - pair[:, 1 - k : 2 - k]
        shares_k.append(chosen * jax.nn.sigmoid(spread_k))

    def r_arrived(d):
        s = (e + d) % E
        for i in range(EL):
            remote(RES.at[s, i], RB.at[s, i], tx_r.at[i, 0], rx_r.at[s, i], s, t).wait_recv()

    loop(E, r_arrived, 1)
    returned = RB[...].reshape(experts * CAP, RB.shape[3])
    combined = shares_k[0] * dot(takes[0], returned) + shares_k[1] * dot(takes[1], returned)
    out_ref[...] = combined.astype(bf16)

    loop(E, lambda d: meta_copy(d).wait_send(), 1)
    loop(Z, lambda d: z_copy(d).wait_send(), 1)
    loop(T, lambda q: mate_copy(e, q).wait_send())

    def sent(d):
        s = 2 * ((z + d) % Z) + c
        loop(T, lambda j: tp_copy(s, j).wait_send(), 1)
        loop(T, lambda q: mate_copy(s, q).wait_send())

        @pl.when((z + d) % Z > z)
        def _():
            kv_copy(d).wait_send()

    loop(Z, sent, 1)
    loop(z, lambda k: kv_mate(2 * k + c).wait_send())

    @pl.when(c == 0)
    def _():
        kv_mate(e).wait_send()

    def sent_expert(i):
        loop(T, lambda j: h_copy(i, j).wait_send(), 1)
        loop(E, lambda d: r_copy(i, d).wait_send(), 1)

    loop(EL, sent_expert)
    loop(T, lambda j: a_copy(j).wait_send(), 1)


def shards(
    E,
    T,
    attn_rows,
    attn_gain,
    query_weight,
    key_weight,
    value_weight,
    key_bias,
    out_weight,
    expert_rows,
    expert_gain,
    expert_ids,
    group_logits,
    pair_logits,
    gate_weight,
    up_weight,
    down_weight,
):
    R, D = attn_rows.shape
    W = query_weight.shape[1]
    heads = key_bias.shape[0]
    HD = W // heads
    EL, _, FL = gate_weight.shape
    DL = down_weight.shape[2]
    Z = E // 2
    DQ = D // T
    meta_rows = BIAS_ROW + -(-heads // 8) * 8
    meta = jnp.concatenate(
        [
            jnp.pad(expert_ids.T.astype(f32), ((0, BIAS_ROW - 2), (0, 0))),
            jnp.pad(key_bias.astype(f32), ((0, meta_rows - BIAS_ROW - heads), (0, 0))),
        ],
        axis=0,
    )
    vmem = pl.BlockSpec(memory_space=pltpu.VMEM)
    hbm = pl.BlockSpec(memory_space=pl.ANY)
    dma = pltpu.SemaphoreType.DMA
    qkv = (D, 3 * W) if W % 128 == 0 else (3, D, W)
    return pl.pallas_call(
        functools.partial(kernel, E, T),
        out_shape=(
            jax.ShapeDtypeStruct((R, out_weight.shape[1]), bf16),
            jax.ShapeDtypeStruct((R, DL), bf16),
        ),
        in_specs=[vmem, vmem, hbm, hbm, hbm, vmem, hbm, hbm, vmem, vmem, vmem, vmem, hbm, hbm, hbm],
        out_specs=(vmem, vmem),
        scratch_shapes=[
            pltpu.VMEM(qkv, bf16),
            pltpu.VMEM(out_weight.shape, bf16),
            pltpu.VMEM(gate_weight.shape, bf16),
            pltpu.VMEM(up_weight.shape, bf16),
            pltpu.VMEM(down_weight.shape, bf16),
            pltpu.VMEM((E, T, R, DQ), bf16),
            pltpu.VMEM((EL, E, CAP, D), bf16),
            pltpu.VMEM((T, EL, E * CAP, FL), bf16),
            pltpu.VMEM((E, meta_rows, R), f32),
            pltpu.VMEM((E, R, 2 * W), bf16),
            pltpu.VMEM((heads, R, HD), bf16),
            pltpu.VMEM((T, R, W), bf16),
            pltpu.VMEM((E, EL, CAP, DL), bf16),
            pltpu.VMEM((E, EL, CAP, DL), bf16),
            dma((4,)),
            dma((EL,)),
            dma((EL,)),
            dma((EL,)),
            dma((T,)),
            dma((Z,)),
            dma((E, T)),
            dma((E, T)),
            dma((E, T)),
            dma((E,)),
            dma((E,)),
            dma((Z,)),
            dma((E,)),
            dma((E,)),
            dma((EL, T)),
            dma((EL, T)),
            dma((T,)),
            dma((T,)),
            dma((EL, E)),
            dma((E, EL)),
        ],
        compiler_params=pltpu.CompilerParams(
            collective_id=0, has_side_effects=True, vmem_limit_bytes=63 * 1024 * 1024
        ),
    )(
        attn_rows,
        attn_gain.reshape(1, D),
        query_weight,
        key_weight,
        value_weight,
        meta,
        out_weight,
        expert_rows,
        expert_gain.reshape(1, D),
        expert_ids,
        group_logits,
        pair_logits,
        gate_weight,
        up_weight,
        down_weight,
    )


def solution(mesh):
    placed = (
        P("ep", None),
        P(),
        P(None, "tp"),
        P(None, "tp"),
        P(None, "tp"),
        P("tp", "ep"),
        P(None, "tp"),
        P("ep", None),
        P(),
        P("ep", None),
        P("ep", None),
        P("ep", None),
        P("ep", None, "tp"),
        P("ep", None, "tp"),
        P("ep", None, "tp"),
    )
    return jax.shard_map(
        functools.partial(shards, mesh.shape["ep"], mesh.shape["tp"]),
        mesh=mesh,
        in_specs=placed,
        out_specs=(P("ep", "tp"), P("ep", "tp")),
        check_vma=False,
    )
```

time: 219 us -> 84.9 us (0.39)
  blocking collectives: 75.8 us -> 0 us
  Pallas kernels: 0 us -> 74.7 us
  local copies, waits for them, and re-layouts: 48.8 us -> 7.37 us
  waiting for transfers between devices: 41.4 us -> 0 us
  matrix products: 16.2 us -> 0 us
  other arithmetic: 16.2 us -> 1.97 us
  between operations: 14.4 us -> 0.64 us
  starting transfers between devices: 4.69 us -> 0 us
    pallas_call x0 -> x1, Pallas kernels: none -> 74.7 us  [shards(): pl.pallas_call(functools.partial(kernel, E, T), out_shape=(jax.ShapeDtype...]
    all_to_all x1 -> x0, blocking collectives: 55.5 us -> none  [shards(): lax.all_to_all(send, 'ep', split_axis=0, concat_axis=0, tiled=True)]
    all_gather x2 -> x0, waiting for transfers between devices: 41.4 us -> none  [the longest x1 21.8 us: shards(): lax.all_gather(hidden, 'tp', axis=3, tiled=True)]
    scatter x1 -> x0, local copies, waits for them, and re-layouts: 33.3 us -> none  [shards(): jnp.zeros((EXPERTS, CAP, width), jnp.bfloat16).at[flattened, position]]
    all_gather x2 -> x0, blocking collectives: 20.4 us -> none  [the longest x1 10.7 us: shards(): lax.all_gather(attended, 'tp', axis=1, tiled=True)]
    dot_general x9 -> x0, matrix products: 16.2 us -> none  [the longest x1 5.28 us: shards(): jnp.einsum('secf,efd->secd', lax.all_gather(hidden, 'tp', axis=3, tiled=T...]
    another operation x4 -> x0, other arithmetic: 8.41 us -> none  [the longest x1 7.74 us: work(): suffix = lax.cumsum(log_keep, axis=3, reverse=True) - log_keep]
    unnamed x25 -> x5, local copies, waits for them, and re-layouts: 1.54 us -> 7.37 us
  transfers between devices with their start and end apart: 3 -> 0, of which waited for: 2 -> 0; matrix products, arithmetic and copies ran while one was open for 13% -> 0% of each run, Pallas kernels for 0% -> 0%
where the time goes in v1:
time: 84.9 us; the launch traced here: 84.7 us
  Pallas kernels  74.7 us (88%)
  local copies, waits for them, and re-layouts  7.37 us (9%)
  other arithmetic  1.97 us (2%)
    pallas_call x1, Pallas kernels, shards(): pl.pallas_call(functools.partial(kernel, E, T), out_shape=(jax.ShapeDtype...  74.7 us
    unnamed x5, local copies, waits for them, and re-layouts  7.37 us

profile of v1, /device:TPU:0, one launch (start us, length us, event | category | flops | bytes accessed | tf_op | source)
XLA Modules:
  0.0 84.7 jit_solution(15734153775031200426)
XLA Ops:
  0.6 0.7 convert_bitcast_fusion
  1.3 0.7 pad_convert_fusion
  2.0 0.6 select_maximum_fusion.meta_ref
  2.6 1.4 %copy.18.glog_ref = f32[128,4]{1,0:T(8,128)} copy(f32[128,4]{0,1:T(4,128)} %param.25) | data formatting | bytes 4096 | tf_op args[10]
  4.0 1.4 %copy.19.plog_ref = f32[128,2]{1,0:T(8,128)} copy(f32[128,2]{0,1:T(2,128)} %param.26) | data formatting | bytes 2048 | tf_op args[11]
  5.4 1.4 %copy.17.ids_ref = s32[128,2]{1,0:T(8,128)} copy(s32[128,2]{0,1:T(2,128)} %param.24) | data formatting | bytes 2048 | tf_op args[9]
  6.8 74.7 %shard_map.158 = (bf16[128,512]{1,0:T(8,128)(2,1)}, bf16[128,512]{1,0:T(8,128)(2,1)}) custom-call(bf16[128,2048]{1,0:T(8,128)(2,1)} %rows_ref.1, f32[1,2048]{1,0:T(1,128)} %bitcast.4, bf16[2048,256]{1,0:T(8,128)(2,1)} %wq_hbm.1, bf16[2048,256]{1,0:T(8,128)(2,1)} %wk_hbm.1, bf16[2048,256]{1,0:T(8,128)(2,1)} %wv_hbm.1, f32[16,128]{1,0:T(8,128)} %select_maximum_fusion.meta_ref, ...), custom_call_target="tpu_custom_call" | custom-call | tf_op jit(solution)/shard_map/pallas_call | solution.py:467
  81.5 1.6 %copy.22 = bf16[128,512]{1,0:T(8,128)(2,1)} copy(bf16[128,512]{1,0:T(8,128)(2,1)} %get-tuple-element.4) | data formatting | bytes 262144
  83.1 1.6 %copy.23 = bf16[128,512]{1,0:T(8,128)(2,1)} copy(bf16[128,512]{1,0:T(8,128)(2,1)} %get-tuple-element.5) | data formatting | bytes 262144

commit v2 on v1

--- a/solution.py
+++ b/solution.py
@@ -37,7 +37,7 @@
     wq_hbm,
     wk_hbm,
     wv_hbm,
-    meta_ref,
+    bias_ref,
     wo_hbm,
     erows_hbm,
     egain_ref,
@@ -63,6 +63,7 @@
     AT,
     RES,
     RB,
+    COL,
     s_w,
     s_wg,
     s_wu,
@@ -83,7 +84,12 @@
     rx_a,
     tx_r,
     rx_r,
+    tx_f,
+    rx_f,
+    tx_hf,
+    rx_hf,
 ):
+    square = T == 4
     Z = E // 2
     R, D = rows_ref.shape
     W = wq_hbm.shape[1]
@@ -160,6 +166,10 @@
     loop(T, greet_tp, 1)
     pl.semaphore_wait(barrier, E - 1 + T - 1)
 
+    M[e] = jnp.zeros(M.shape[1:], f32)
+    M[e, 0:2, :] = ids_ref[...].astype(f32)
+    M[e, BIAS_ROW : BIAS_ROW + heads, :] = bias_ref[...].astype(f32)
+
     for cp in x_copies:
         cp.wait()
 
@@ -171,13 +181,33 @@
     def mate_copy(s, q):
         return remote(X.at[s, q], X.at[s, q], tx_d.at[s, q], rx.at[s, q], mate, t)
 
-    def tp_copy(s, j):
-        return remote(
-            X.at[s, t], X.at[s, t], tx_tp.at[s, j], rx.at[s, t], e, (t + j) % T
-        )
+    side, down_side, far = t - t % 2 + 1 - t % 2, (t + 2) % 4, 3 - t
+    peers = [side, down_side] if square else [(t + j) % T for j in range(1, T)]
+    half = R // 2
+
+    def to_peers(make):
+        for j, peer in enumerate(peers):
+            make(j, peer)
+
+    def tp_copy(s, j, peer):
+        return remote(X.at[s, t], X.at[s, t], tx_tp.at[s, j], rx.at[s, t], e, peer)
+
+    def pass_first(s):
+        part = X.at[s, side, pl.ds(0, half)]
+        return remote(part, part, tx_f.at[s, 0], rx.at[s, side], e, down_side)
+
+    def pass_second(s):
+        part = X.at[s, down_side, pl.ds(half, R - half)]
+        return remote(part, part, tx_f.at[s, 1], rx_f.at[s], e, side)
+
+    def far_arrived(s):
+        part = X.at[s, far, pl.ds(0, half)]
+        remote(part, part, tx_f.at[s, 0], rx.at[s, far], e, t).wait_recv()
+        part = X.at[s, far, pl.ds(half, R - half)]
+        remote(part, part, tx_f.at[s, 1], rx_f.at[s], e, t).wait_recv()
 
     def meta_copy(d):
-        return remote(meta_ref, M.at[e], tx_m.at[d], rx_m.at[e], (e + d) % E, t)
+        return remote(M.at[e], M.at[e], tx_m.at[d], rx_m.at[e], (e + d) % E, t)
 
     def kv_copy(d):
         return remote(
@@ -190,10 +220,9 @@
     def x_arrived(s, q):
         mate_copy(s, q).wait_recv()
 
+    loop(Z, lambda d: z_copy(d).start(), 1)
     loop(E, lambda d: meta_copy(d).start(), 1)
-    loop(Z, lambda d: z_copy(d).start(), 1)
     loop(T, lambda q: mate_copy(e, q).start())
-    M[e] = meta_ref[...]
 
     values = rows_ref[...].astype(f32)
     scaled = values * lax.rsqrt(jnp.mean(values * values, axis=-1, keepdims=True) + epsilon)
@@ -205,6 +234,18 @@
     else:
         KV[e] = jnp.concatenate([dot(normed, wqkv[0]), dot(normed, wqkv[1])], axis=1).astype(bf16)
 
+    query = dot(normed, wqkv[:, 2 * W :] if W % 128 == 0 else wqkv[2]).astype(bf16)
+    for h in range(heads):
+        Q[h] = query[:, h * HD : (h + 1) * HD]
+
+    def relay(d):
+        s = 2 * ((z + d) % Z) + c
+        x_arrived(s, t)
+        to_peers(lambda j, peer: tp_copy(s, j, peer).start())
+        mate_copy(s, t).start()
+
+    loop(Z, relay, 1)
+
     def kv_send(d):
         @pl.when((z + d) % Z > z)
         def _():
@@ -216,17 +257,6 @@
     def _():
         kv_mate(e).start()
 
-    query = dot(normed, wqkv[:, 2 * W :] if W % 128 == 0 else wqkv[2]).astype(bf16)
-    for h in range(heads):
-        Q[h] = query[:, h * HD : (h + 1) * HD]
-
-    def relay(d):
-        s = 2 * ((z + d) % Z) + c
-        x_arrived(s, t)
-        loop(T, lambda j: tp_copy(s, j).start(), 1)
-        mate_copy(s, t).start()
-
-    loop(Z, relay, 1)
 
     row_i = lax.broadcasted_iota(jnp.int32, (R, R), 0)
     col_i = lax.broadcasted_iota(jnp.int32, (R, R), 1)
@@ -250,39 +280,68 @@
             for i in range(EL):
                 XG[i, s, :, pl.ds(q * DQ, DQ)] = part[i * CAP : (i + 1) * CAP]
 
-    loop(E, lambda d: remote(meta_ref, M.at[(e + d) % E], tx_m.at[0], rx_m.at[(e + d) % E], e, t).wait_recv(), 1)
+    loop(E, lambda d: remote(M.at[(e + d) % E], M.at[(e + d) % E], tx_m.at[0], rx_m.at[(e + d) % E], e, t).wait_recv(), 1)
     pick(e)
 
     def mate_rows(s):
         loop(T, lambda q: x_arrived(s, q))
         pick(s)
 
-    mate_rows(mate)
-
     def kv_relay(s):
         kv_mate(s).wait_recv()
         kv_mate(s).start()
 
+    if square:
+
+        def forward(d):
+            s = 2 * ((z + d) % Z) + c
+            x_arrived(s, side)
+            pass_first(s).start()
+            mate_copy(s, side).start()
+            x_arrived(s, down_side)
+            pass_second(s).start()
+            mate_copy(s, down_side).start()
+
+        loop(Z, forward, 1)
+
+    mate_rows(mate)
     loop(z, lambda k: kv_relay(2 * k + c))
 
     def spread(d):
         s = 2 * ((z + d) % Z) + c
-
-        def on(j):
-            q = (t + j) % T
-            x_arrived(s, q)
-            mate_copy(s, q).start()
-
-        loop(T, on, 1)
+        if square:
+            far_arrived(s)
+            mate_copy(s, far).start()
+        else:
+            for q in peers:
+                x_arrived(s, q)
+                mate_copy(s, q).start()
         pick(s)
 
     loop(Z, spread, 1)
     loop(Z, lambda d: mate_rows(2 * ((z + d) % Z) + (1 - c)), 1)
 
-    def h_copy(i, j):
-        return remote(
-            HB.at[t, i], HB.at[t, i], tx_h.at[i, j], rx_h.at[i, t], e, (t + j) % T
-        )
+    def h_copy(i, j, peer):
+        return remote(HB.at[t, i], HB.at[t, i], tx_h.at[i, j], rx_h.at[i, t], e, peer)
+
+    def h_arrived(i, q):
+        remote(HB.at[q, i], HB.at[q, i], tx_h.at[i, 0], rx_h.at[i, q], e, t).wait_recv()
+
+    h_half = E * CAP // 2
+
+    def h_first(i, q, peer):
+        part = HB.at[q, i, pl.ds(0, h_half)]
+        return remote(part, part, tx_hf.at[i, 0], rx_h.at[i, q], e, peer)
+
+    def h_second(i, q, peer):
+        part = HB.at[q, i, pl.ds(h_half, h_half)]
+        return remote(part, part, tx_hf.at[i, 1], rx_hf.at[i], e, peer)
+
+    def h_forward(i):
+        h_arrived(i, side)
+        h_first(i, side, down_side).start()
+        h_arrived(i, down_side)
+        h_second(i, down_side, side).start()
 
     def hidden(i):
         rows = XG[i].reshape(E * CAP, D)
@@ -291,9 +350,12 @@
         wu_copy(i).wait()
         up = dot(rows, wu[i])
         HB[t, i] = (jax.nn.silu(gate) * up).astype(bf16)
-        loop(T, lambda j: h_copy(i, j).start(), 1)
-
-    loop(EL, hidden)
+        to_peers(lambda j, peer: h_copy(i, j, peer).start())
+
+    for i in range(EL):
+        hidden(i)
+        if square and i >= 2:
+            h_forward(i - 2)
 
     loop(z, lambda k: kv_mate(2 * k + (1 - c)).wait_recv())
 
@@ -301,34 +363,41 @@
     def _():
         kv_mate(mate).wait_recv()
 
-    def block(j, carry):
-        s = e - j
-        causal = col_i + s * R < row_i + e * R
-        new = []
-        for h in range(heads):
-            later, total = carry[h]
-            key = KV[s, :, pl.ds(h * HD, HD)]
-            value = KV[s, :, pl.ds(W + h * HD, HD)]
-            score = lax.dot_general(
-                Q[h], key, (((1,), (1,)), ((), ())), preferred_element_type=f32
-            )
-            score = score * scale + M[s, pl.ds(BIAS_ROW + h, 1), :]
-            negative = -(jnp.maximum(score, 0.0) + jnp.log1p(jnp.exp(-jnp.abs(score))))
-            keep = jnp.where(causal, negative, 0.0)
-            high = keep.astype(bf16)
-            low = (keep - high.astype(f32)).astype(bf16)
-            suffix = dot(high, after) + dot(low, after)
-            weight = jnp.where(causal, jnp.exp(score + negative + suffix), 0.0).astype(bf16)
-            total = total + jnp.exp(later) * dot(weight, value)
-            later = later + suffix[:, 0:1] + keep[:, 0:1]
-            new.append((later, total))
-        return tuple(new)
-
-    init = tuple(
-        (jnp.zeros((R, 1), f32), jnp.zeros((R, HD), f32)) for _ in range(heads)
-    )
-    merged = lax.fori_loop(0, e + 1, block, init)
-    AT[t] = jnp.concatenate([total for _, total in merged], axis=1).astype(bf16)
+    def attend(group):
+        def block(j, carry):
+            s = e - j
+            causal = col_i + s * R < row_i + e * R
+            new = []
+            for h, (later, total) in zip(group, carry):
+                key = KV[s, :, pl.ds(h * HD, HD)]
+                value = KV[s, :, pl.ds(W + h * HD, HD)]
+                score = lax.dot_general(
+                    Q[h], key, (((1,), (1,)), ((), ())), preferred_element_type=f32
+                )
+                score = score * scale + M[s, pl.ds(BIAS_ROW + h, 1), :]
+                negative = -(jnp.maximum(score, 0.0) + jnp.log1p(jnp.exp(-jnp.abs(score))))
+                keep = jnp.where(causal, negative, 0.0)
+                high = keep.astype(bf16)
+                low = (keep - high.astype(f32)).astype(bf16)
+                suffix = dot(high, after) + dot(low, after)
+                weight = jnp.where(causal, jnp.exp(score + negative + suffix), 0.0).astype(bf16)
+                total = total + jnp.exp(later) * dot(weight, value)
+                later = later + suffix[:, 0:1] + keep[:, 0:1]
+                new.append((later, total))
+            return tuple(new)
+
+        init = tuple((jnp.zeros((R, 1), f32), jnp.zeros((R, HD), f32)) for _ in group)
+        return [total for _, total in lax.fori_loop(0, e + 1, block, init)]
+
+    attended = []
+    late = list(range(max(EL - 2, 0), EL)) if square else []
+    for first in range(0, heads, 2):
+        attended += attend(list(range(first, min(first + 2, heads))))
+        if late:
+            h_forward(late.pop(0))
+    for i in late:
+        h_forward(i)
+    AT[t] = jnp.concatenate(attended, axis=1).astype(bf16)
 
     def a_copy(j):
         return remote(AT.at[t], AT.at[t], tx_a.at[j], rx_a.at[t], e, (t + j) % T)
@@ -342,11 +411,12 @@
     def down(i):
         wd_copy(i).wait()
 
-        def arrived(j):
-            q = (t + j) % T
-            remote(HB.at[q, i], HB.at[q, i], tx_h.at[i, 0], rx_h.at[i, q], e, t).wait_recv()
-
-        loop(T, arrived, 1)
+        if square:
+            h_first(i, far, t).wait_recv()
+            h_second(i, far, t).wait_recv()
+        else:
+            for q in peers:
+                h_arrived(i, q)
         result = dot(HB[0, i], wd[i, pl.ds(0, FL), :])
         for q in range(1, T):
             result = result + dot(HB[q, i], wd[i, pl.ds(q * FL, FL), :])
@@ -370,15 +440,21 @@
     mixed_ref[...] = mixed.astype(bf16)
 
     experts = E * EL
-    ids = [ids_ref[:, k : k + 1] for k in range(2)]
+    groups = glog_ref.shape[0]
+    COL[...] = jnp.zeros(COL.shape, f32)
+    COL[0:2, :] = ids_ref[...].astype(f32)
+    COL[2 : 2 + groups, :] = glog_ref[...]
+    COL[2 + groups : 4 + groups, :] = plog_ref[...]
+    columns = COL[...].T
+    ids = [columns[:, k : k + 1].astype(jnp.int32) for k in range(2)]
     expert_i = lax.broadcasted_iota(jnp.int32, (R, experts), 1)
     named = (expert_i == ids[0]) | (expert_i == ids[1])
     places = dot(after, named.astype(f32).astype(bf16))
-    shares = jnp.exp(glog_ref[...])
+    shares = jnp.exp(columns[:, 2 : 2 + groups])
     shares = shares / jnp.sum(shares, axis=1, keepdims=True)
     group_i = lax.broadcasted_iota(jnp.int32, shares.shape, 1)
     back_i = lax.broadcasted_iota(jnp.int32, (R, experts * CAP), 1)
-    pair = plog_ref[...]
+    pair = columns[:, 2 + groups : 4 + groups]
     takes, shares_k = [], []
     for k in range(2):
         own = jnp.sum(jnp.where(expert_i == ids[k], places, 0.0), axis=1, keepdims=True)
@@ -403,7 +479,10 @@
 
     def sent(d):
         s = 2 * ((z + d) % Z) + c
-        loop(T, lambda j: tp_copy(s, j).wait_send(), 1)
+        to_peers(lambda j, peer: tp_copy(s, j, peer).wait_send())
+        if square:
+            pass_first(s).wait_send()
+            pass_second(s).wait_send()
         loop(T, lambda q: mate_copy(s, q).wait_send())
 
         @pl.when((z + d) % Z > z)
@@ -418,11 +497,19 @@
         kv_mate(e).wait_send()
 
     def sent_expert(i):
-        loop(T, lambda j: h_copy(i, j).wait_send(), 1)
+        to_peers(lambda j, peer: h_copy(i, j, peer).wait_send())
+        if square:
+            h_first(i, side, down_side).wait_send()
+            h_second(i, down_side, side).wait_send()
         loop(E, lambda d: r_copy(i, d).wait_send(), 1)
 
     loop(EL, sent_expert)
     loop(T, lambda j: a_copy(j).wait_send(), 1)
+
+
+def write_results(mixed_ref, out_ref, mixed_to, out_to):
+    mixed_to[...] = mixed_ref[...]
+    out_to[...] = out_ref[...]
 
 
 def shards(
@@ -453,18 +540,12 @@
     Z = E // 2
     DQ = D // T
     meta_rows = BIAS_ROW + -(-heads // 8) * 8
-    meta = jnp.concatenate(
-        [
-            jnp.pad(expert_ids.T.astype(f32), ((0, BIAS_ROW - 2), (0, 0))),
-            jnp.pad(key_bias.astype(f32), ((0, meta_rows - BIAS_ROW - heads), (0, 0))),
-        ],
-        axis=0,
-    )
+    col_rows = -(-(4 + group_logits.shape[1]) // 8) * 8
     vmem = pl.BlockSpec(memory_space=pltpu.VMEM)
     hbm = pl.BlockSpec(memory_space=pl.ANY)
     dma = pltpu.SemaphoreType.DMA
     qkv = (D, 3 * W) if W % 128 == 0 else (3, D, W)
-    return pl.pallas_call(
+    results = pl.pallas_call(
         functools.partial(kernel, E, T),
         out_shape=(
             jax.ShapeDtypeStruct((R, out_weight.shape[1]), bf16),
@@ -487,6 +568,7 @@
             pltpu.VMEM((T, R, W), bf16),
             pltpu.VMEM((E, EL, CAP, DL), bf16),
             pltpu.VMEM((E, EL, CAP, DL), bf16),
+            pltpu.VMEM((col_rows, R), f32),
             dma((4,)),
             dma((EL,)),
             dma((EL,)),
@@ -507,6 +589,10 @@
             dma((T,)),
             dma((EL, E)),
             dma((E, EL)),
+            dma((E, 2)),
+            dma((E,)),
+            dma((EL, 2)),
+            dma((EL,)),
         ],
         compiler_params=pltpu.CompilerParams(
             collective_id=0, has_side_effects=True, vmem_limit_bytes=63 * 1024 * 1024
@@ -517,17 +603,23 @@
         query_weight,
         key_weight,
         value_weight,
-        meta,
+        key_bias,
         out_weight,
         expert_rows,
         expert_gain.reshape(1, D),
-        expert_ids,
-        group_logits,
-        pair_logits,
+        expert_ids.T,
+        group_logits.T,
+        pair_logits.T,
         gate_weight,
         up_weight,
         down_weight,
     )
+    return pl.pallas_call(
+        write_results,
+        out_shape=tuple(jax.ShapeDtypeStruct(r.shape, r.dtype) for r in results),
+        in_specs=[vmem, vmem],
+        out_specs=(vmem, vmem),
+    )(*results)
 
 
 def solution(mesh):

time: 84.9 us -> 71.8 us (0.85)
  local copies, waits for them, and re-layouts: 7.37 us -> 0 us
  Pallas kernels: 74.7 us -> 71 us
  other arithmetic: 1.97 us -> 0 us
    unnamed x5 -> x0, local copies, waits for them, and re-layouts: 7.37 us -> none
    pallas_call x1, Pallas kernels: 74.7 us -> 69.3 us  [shards(): pl.pallas_call(functools.partial(kernel, E, T), out_shape=(jax.ShapeDtype...]
    pallas_call x0 -> x1, Pallas kernels: none -> 1.68 us  [shards(): pl.pallas_call(write_results, out_shape=tuple((jax.ShapeDtypeStruct(r.sha...]
where the time goes in v2:
time: 71.8 us; the launch traced here: 71.6 us
  Pallas kernels  71 us (99%)
    pallas_call x1, Pallas kernels, shards(): pl.pallas_call(functools.partial(kernel, E, T), out_shape=(jax.ShapeDtype...  69.3 us
    pallas_call x1, Pallas kernels, shards(): pl.pallas_call(write_results, out_shape=tuple((jax.ShapeDtypeStruct(r.sha...  1.68 us

profile of v2, /device:TPU:0, one launch (start us, length us, event | category | flops | bytes accessed | tf_op | source)
XLA Modules:
  0.0 71.6 jit_solution(16985474446660182837)
XLA Ops:
  0.6 69.3 %shard_map.158 = (bf16[128,512]{1,0:T(8,128)(2,1)}, bf16[128,512]{1,0:T(8,128)(2,1)}) custom-call(bf16[128,2048]{1,0:T(8,128)(2,1)} %rows_ref.1, f32[1,2048]{1,0:T(1,128)} %bitcast.5, bf16[2048,256]{1,0:T(8,128)(2,1)} %wq_hbm.1, bf16[2048,256]{1,0:T(8,128)(2,1)} %wk_hbm.1, bf16[2048,256]{1,0:T(8,128)(2,1)} %wv_hbm.1, bf16[4,128]{1,0:T(4,128)(2,1)} %bias_ref.1, ...), custom_call_target="tpu_custom_call" | custom-call | tf_op jit(solution)/shard_map/pallas_call | solution.py:548
  70.0 1.7 %shard_map.159 = (bf16[128,512]{1,0:T(8,128)(2,1)}, bf16[128,512]{1,0:T(8,128)(2,1)}) custom-call(bf16[128,512]{1,0:T(8,128)(2,1)} %get-tuple-element.4.mixed_ref, bf16[128,512]{1,0:T(8,128)(2,1)} %get-tuple-element.5.out_ref), custom_call_target="tpu_custom_call" | custom-call | tf_op jit(solution)/shard_map/pallas_call | solution.py:617
